TPU v7x, 32 devices: a whole 2x2x4 slice. The times are simulated.
32 devices in a mesh: grp: 2 (over y), sp: 4 (over z), tp: 4 (over x, core).
Axes of the slice: x: 2, y: 2, z: 4, core: 2. Of those that a mesh axis runs over, the one named last changes fastest.
Arguments:
- resid_in: bfloat16 [2048, 2048], P(('grp', 'sp', 'tp')), parts along dimension 0, may hold values from -6 to 6
- query_narrow: bfloat16 [2048, 8, 128], P(('grp', 'sp'), 'tp'), parts along dimension 0, may hold values from -512 to 512
- key_narrow: bfloat16 [2048, 4, 128], P(('grp', 'sp'), 'tp'), parts along dimension 0, may hold values from -512 to 512
- value_narrow: bfloat16 [2048, 4, 128], P(('grp', 'sp'), 'tp'), parts along dimension 0, may hold values from -6 to 6
- query_wide: bfloat16 [2048, 8, 256], P(('grp', 'sp'), 'tp'), parts along dimension 0, may hold values from -512 to 512
- key_wide: bfloat16 [2048, 4, 256], P(('grp', 'sp'), 'tp'), parts along dimension 0, may hold values from -512 to 512
- value_wide: bfloat16 [2048, 4, 128], P(('grp', 'sp'), 'tp'), parts along dimension 0, may hold values from -6 to 6
- lambda_narrow: float32 [8], P('tp'), may hold values from 0.3 to 0.8
- lambda_wide: float32 [8], P('tp'), may hold values from 0.3 to 0.8
- head_gain: float32 [128], replicated, may hold values from 0.1 to 1.9
- out_narrow: bfloat16 [1024, 2048], P('tp'), may hold values from -0.125 to 0.125
- out_wide: bfloat16 [1024, 2048], P('tp'), may hold values from -0.125 to 0.125
- norm_gain: bfloat16 [2048], replicated, may hold values from 0.099609375 to 1.8984375
- up_weight: bfloat16 [2048, 8192], P('sp', 'tp'), may hold values from -0.125 to 0.125
- down_weight: bfloat16 [8192, 2048], P('tp', 'sp'), may hold values from -0.0625 to 0.0625
Outputs:
- mixed_out: bfloat16 [2048, 2048], P(('grp', 'sp', 'tp')), parts along dimension 0
There are 2 independent parts, one for each index of `grp`. A program takes and returns all parts, laid end to end along the dimension named above; an argument that names none is the same for every part. Nothing has to cross between parts.
All inputs are finite; a program needn't handle non-finite values.
Results may differ from a plain program's by a relative error of at most 0.018.
Values may be sent and summed in bfloat16 or wider, within the bound.
A program may use at most 128 MiB of HBM per device.

v0:
```python
import math

import jax
import jax.numpy as jnp
from jax import lax
from jax.sharding import PartitionSpec as P

NORM_EPS = 1e-06
OUT_SCALE = 0.8


def empty_state(query, key_head_stack, value_width):
    row_count, head_count = (query.shape[0], query.shape[1])
    group_size = head_count // key_head_stack
    row_top = jnp.full((key_head_stack, group_size, 2, row_count), -jnp.inf, jnp.float32)
    row_total = jnp.zeros((key_head_stack, group_size, 2, row_count), jnp.float32)
    weighted_values = jnp.zeros(
        (key_head_stack, group_size, 2, row_count, value_width), jnp.float32
    )
    return (row_top, row_total, weighted_values)


def absorb(states, query, key_rows, values):
    row_count, head_count = (query.shape[0], query.shape[1])
    key_head_stack = key_rows.shape[1]
    half_width = key_rows.shape[2] // 2
    group_size = head_count // key_head_stack
    value_width = values.shape[2]
    amount = key_rows.shape[0]
    block_rows = math.gcd(amount, 512)
    rotation_count = amount // block_rows
    grouped = query.reshape(row_count, key_head_stack, group_size, 2, half_width)
    key_block_list = key_rows.reshape(rotation_count, block_rows, key_head_stack, 2, half_width)
    value_blocks = values.reshape(rotation_count, block_rows, key_head_stack, value_width)

    def visit(running, kv_pair):
        row_top, row_total, weighted_values = running
        key_blk, value_blk = kv_pair
        scores = jnp.einsum(
            "tkgcd,skcd->kgcts", grouped, key_blk, preferred_element_type=jnp.float32
        ) * half_width ** (-0.5)
        new_top = jnp.maximum(row_top, jnp.max(scores, axis=-1))
        rescale = jnp.exp(row_top - new_top)
        powers = jnp.exp(scores - new_top[..., None])
        row_total = row_total * rescale + jnp.sum(powers, axis=-1)
        weighted_values = weighted_values * rescale[..., None] + jnp.einsum(
            "iodph,hie->iodpe",
            powers.astype(jnp.bfloat16),
            value_blk,
            preferred_element_type=jnp.float32,
        )
        return ((new_top, row_total, weighted_values), None)

    outcome, _ = lax.scan(visit, states, (key_block_list, value_blocks))
    return outcome


def finish(states, lambdas, gain_vec):
    row_top, row_total, weighted_values = states
    key_head_stack, group_size, row_count = (row_top.shape[0], row_top.shape[1], row_top.shape[3])
    value_width = weighted_values.shape[4]
    first_map = weighted_values[:, :, 0] / row_total[:, :, 0, :, None]
    second_map = weighted_values[:, :, 1] / row_total[:, :, 1, :, None]
    mixed = first_map - lambdas.reshape(key_head_stack, group_size)[:, :, None, None] * second_map
    normed = (
        mixed
        * lax.rsqrt(jnp.mean(mixed * mixed, axis=-1, keepdims=True) + NORM_EPS)
        * gain_vec
        * OUT_SCALE
    )
    normed = normed.astype(jnp.bfloat16).transpose(2, 0, 1, 3)
    return normed.reshape(row_count, key_head_stack * group_size * value_width)


def attend(
    query_narrow,
    key_narrow,
    value_narrow,
    query_wide,
    key_wide,
    value_wide,
    lambda_narrow,
    lambda_wide,
    head_gain,
):
    initial = (
        empty_state(query_narrow, key_narrow.shape[1], value_narrow.shape[2]),
        empty_state(query_wide, key_wide.shape[1], value_wide.shape[2]),
    )
    narrow_keys = lax.all_gather(key_narrow, "sp", axis=0, tiled=True)
    narrow_values = lax.all_gather(value_narrow, "sp", axis=0, tiled=True)
    wide_keys = lax.all_gather(key_wide, "sp", axis=0, tiled=True)
    wide_values = lax.all_gather(value_wide, "sp", axis=0, tiled=True)
    narrow_state = absorb(initial[0], query_narrow, narrow_keys, narrow_values)
    wide_state = absorb(initial[1], query_wide, wide_keys, wide_values)
    return (
        finish(narrow_state, lambda_narrow, head_gain),
        finish(wide_state, lambda_wide, head_gain),
    )


def shards(
    resid_in,
    query_narrow,
    key_narrow,
    value_narrow,
    query_wide,
    key_wide,
    value_wide,
    lambda_narrow,
    lambda_wide,
    head_gain,
    out_narrow,
    out_wide,
    norm_gain,
    up_weight,
    down_weight,
):
    att_narrow, att_wide = attend(
        query_narrow,
        key_narrow,
        value_narrow,
        query_wide,
        key_wide,
        value_wide,
        lambda_narrow,
        lambda_wide,
        head_gain,
    )
    projected = lax.psum_scatter(
        (
            jnp.dot(att_narrow, out_narrow, preferred_element_type=jnp.float32)
            + jnp.dot(att_wide, out_wide, preferred_element_type=jnp.float32)
        ).astype(jnp.bfloat16),
        "tp",
        scatter_dimension=0,
        tiled=True,
    ).astype(jnp.float32)
    middle = (resid_in.astype(jnp.float32) + projected).astype(jnp.bfloat16)
    middle_f32 = middle.astype(jnp.float32)
    normed = middle_f32 * lax.rsqrt(
        jnp.mean(middle_f32 * middle_f32, axis=-1, keepdims=True) + NORM_EPS
    )
    normed = (normed * norm_gain.astype(jnp.float32)).astype(jnp.bfloat16)
    whole_rows = lax.all_gather(normed, "tp", axis=0, tiled=True)
    up_collected = lax.all_gather(up_weight, "sp", axis=0, tiled=True)
    lifted = jnp.dot(whole_rows, up_collected, preferred_element_type=jnp.float32)
    activated = jnp.square(jax.nn.relu(lifted)).astype(jnp.bfloat16)
    partials = jnp.dot(
        activated,
        lax.all_gather(down_weight, "sp", axis=1, tiled=True),
        preferred_element_type=jnp.float32,
    )
    mixer_out = lax.psum_scatter(
        partials.astype(jnp.bfloat16), "tp", scatter_dimension=0, tiled=True
    ).astype(jnp.float32)
    return (middle_f32 + mixer_out).astype(jnp.bfloat16)


def solution(mesh):
    placed = (
        P(("grp", "sp", "tp"), None),
        P(("grp", "sp"), "tp", None),
        P(("grp", "sp"), "tp", None),
        P(("grp", "sp"), "tp", None),
        P(("grp", "sp"), "tp", None),
        P(("grp", "sp"), "tp", None),
        P(("grp", "sp"), "tp", None),
        P("tp"),
        P("tp"),
        P(),
        P("tp", None),
        P("tp", None),
        P(),
        P("sp", "tp"),
        P("tp", "sp"),
    )
    return jax.shard_map(
        shards, mesh=mesh, in_specs=placed, out_specs=P(("grp", "sp", "tp"), None), check_vma=False
    )
```

profile of v0, /device:TPU:0, one launch (start us, length us, event | category | flops | bytes accessed | tf_op | source)
XLA Modules:
  0.0 480.9 jit_solution(12649065433829812458)
XLA Ops:
  6.6 17.7 %all_gather.23 = bf16[1024,1,256]{2,0,1:T(8,128)(2,1)S(1)} all-gather(bf16[256,1,256]{2,0,1:T(8,128)(2,1)} %param.24), channel_id=1, replica_groups=mesh['grp'=2,'sp'=4,'tp'=4] {'sp'}, dimensions={0}, use_global_device_ids=true | all-gather | bytes 655360 | tf_op jit(solution)/shard_map/all_gather | solution.py:92
  24.4 1.1 copy.33
  25.7 15.3 %all_gather.24 = bf16[1024,1,128]{2,0,1:T(8,128)(2,1)} all-gather(bf16[256,1,128]{2,0,1:T(8,128)(2,1)S(1)} %copy-done.9), channel_id=1, replica_groups=mesh['grp'=2,'sp'=4,'tp'=4] {'sp'}, dimensions={0}, use_global_device_ids=true | all-gather | bytes 327680 | tf_op jit(solution)/shard_map/all_gather | solution.py:93
  41.1 8.2 %while.31 = (s32[]{:T(128)}, f32[1,2,2,256]{3,1,2,0:T(2,128)S(1)}, f32[1,2,2,256]{3,1,2,0:T(2,128)S(1)}, f32[1,2,2,256,128]{4,3,2,1,0:T(8,128)}, bf16[2,512,1,2,...) while((s32[]{:T(128)}, f32[1,2,2,256]{3,1,2,0:T(2,128)S(1)}, ...), condition=%wide.region_8.9_spmd.clone, body=%wide.region_5.0_spmd.clone.sunk | while | flops 271980544 | bytes 13832389 | solution.py:54
  41.3 0.6 copy-done.1
  43.3 1.3 fusion.72
  44.9 0.6 copy-done.1
  46.9 2.3 fusion.72
  49.3 0.6 slice_bitcast_fusion.5
  49.9 14.2 %all_gather.21 = bf16[1024,1,128]{2,0,1:T(8,128)(2,1)S(1)} all-gather(bf16[256,1,128]{2,0,1:T(8,128)(2,1)S(1)} %copy-done.10), channel_id=1, replica_groups=mesh['grp'=2,'sp'=4,'tp'=4] {'sp'}, dimensions={0}, use_global_device_ids=true | all-gather | bytes 327680 | tf_op jit(solution)/shard_map/all_gather | solution.py:90
  64.7 15.6 %all_gather.22 = bf16[1024,1,128]{2,0,1:T(8,128)(2,1)} all-gather(bf16[256,1,128]{2,0,1:T(8,128)(2,1)} %param.22), channel_id=1, replica_groups=mesh['grp'=2,'sp'=4,'tp'=4] {'sp'}, dimensions={0}, use_global_device_ids=true | all-gather | bytes 327680 | tf_op jit(solution)/shard_map/all_gather | solution.py:91
  80.5 6.6 %while.30 = (s32[]{:T(128)}, f32[1,2,2,256]{3,1,2,0:T(2,128)S(1)}, f32[1,2,2,256]{3,1,2,0:T(2,128)S(1)}, f32[1,2,2,256,128]{4,3,2,1,0:T(8,128)}, bf16[2,512,1,2,...) while((s32[]{:T(128)}, f32[1,2,2,256]{3,1,2,0:T(2,128)S(1)}, ...), condition=%wide.region_3.4_spmd.clone, body=%wide.region_0.3_spmd.clone.sunk | while | flops 204871680 | bytes 8851597 | solution.py:54
  80.5 0.5 bitcast_reduce_fusion.4
  81.5 0.5 copy-done.6
  82.0 1.3 fusion.67
  84.3 0.5 copy-done.6
  84.8 2.3 fusion.67
  87.2 1.2 copy.36
  88.5 1.2 copy.31
  90.6 0.6 copy-done.5
  91.2 1.4 fusion.29
  92.7 25.0 %reduce-scatter.3.cloned.1.call-done = bf16[64,2048]{1,0:T(8,128)(2,1)} async-done(((bf16[256,2048]{1,0:T(8,128)(2,1)}), bf16[64,2048]{1,0:T(8,128)(2,1)}) %reduce-scatter.3.cloned.1.call-update) | async-done | bytes 262160 | tf_op jit(solution)/shard_map/reduce_scatter | solution.py:130
  117.7 1.1 fusion.30
  118.8 1.8 fusion.32
  120.7 0.7 all-gather.6.cloned.1.call-update
  121.4 0.5 all-gather.8.cloned.1.call-update
  122.0 15.5 %all-gather.4.cloned.1.call-done = bf16[256,2048]{1,0:T(8,128)(2,1)} async-done(((bf16[64,2048]{1,0:T(8,128)(2,1)}), bf16[256,2048]{1,0:T(8,128)(2,1)}) %all-gather.4.cloned.1.call-update) | async-done | bytes 1048592 | tf_op jit(solution)/shard_map/all_gather | solution.py:145
  137.4 151.2 %all-gather.6.cloned.1.call-done = bf16[2048,2048]{1,0:T(8,128)(2,1)} async-done(((bf16[512,2048]{1,0:T(8,128)(2,1)}), bf16[2048,2048]{1,0:T(8,128)(2,1)}) %all-gather.6.cloned.1.call-update) | async-done | bytes 8388624 | tf_op jit(solution)/shard_map/all_gather | solution.py:146
  288.7 149.3 %all-gather.8.cloned.1.call-done = bf16[2048,2048]{1,0:T(8,128)(2,1)} async-done(((bf16[2048,512]{1,0:T(8,128)(2,1)}), bf16[2048,2048]{1,0:T(8,128)(2,1)}) %all-gather.8.cloned.1.call-update) | async-done | bytes 8388624 | tf_op jit(solution)/shard_map/all_gather | solution.py:151
  437.9 11.5 %convolution_convert_fusion = bf16[256,2048]{1,0:T(8,128)(2,1)} fusion(bf16[2048,2048]{1,0:T(8,128)(2,1)} %all-gather.8.cloned.1.call-done, bf16[256,2048]{1,0:T(8,128)(2,1)} %all-gather.4.cloned.1.call-done, bf16[2048,2048]{1,0:T(8,128)(2,1)} %all-gather.6.cloned.1.call-done), kind=kOutput, calls=%fused_computation.52 | convolution fusion | flops 4297064448 | bytes 18874368 | tf_op jit(solution)/shard_map/dot_general | solution.py:149
  449.5 23.1 %reduce-scatter.5.cloned.1.call-done = bf16[64,2048]{1,0:T(8,128)(2,1)} async-done(((bf16[256,2048]{1,0:T(8,128)(2,1)}), bf16[64,2048]{1,0:T(8,128)(2,1)}) %reduce-scatter.5.cloned.1.call-update) | async-done | bytes 262160 | tf_op jit(solution)/shard_map/reduce_scatter | solution.py:154
  472.6 1.7 fusion.33
  (88 shorter events, 6.6 us)
Async XLA Ops:
  6.5 83.6 %copy-start = (bf16[256,2048]{1,0:T(8,128)(2,1)S(1)}, bf16[256,2048]{1,0:T(8,128)(2,1)}, u32[]{:S(2)}) copy-start(bf16[256,2048]{1,0:T(8,128)(2,1)} %param.29) | copy-start | bytes 3145732
  6.5 19.2 %copy-start.9 = (bf16[256,1,128]{2,0,1:T(8,128)(2,1)S(1)}, bf16[256,1,128]{2,0,1:T(8,128)(2,1)}, u32[]{:S(2)}) copy-start(bf16[256,1,128]{2,0,1:T(8,128)(2,1)} %param.25) | copy-start | bytes 196612
  6.5 111.1 %reduce-scatter.3.cloned.1.call-start = ((), (), s32[]{:S(2)}) async-start(), calls=%async_computation.2 | async-start | bytes 1310720 | tf_op jit(solution)/shard_map/reduce_scatter | solution.py:130
  41.1 8.8 %copy-start.10 = (bf16[256,1,128]{2,0,1:T(8,128)(2,1)S(1)}, bf16[256,1,128]{2,0,1:T(8,128)(2,1)}, u32[]{:S(2)}) copy-start(bf16[256,1,128]{2,0,1:T(8,128)(2,1)} %param.21) | copy-start | bytes 196612
  41.1 0.8 copy-start.1
  42.4 1.0 copy-start.7
  42.8 1.8 copy-start.2
  44.7 0.8 copy-start.1
  45.9 1.0 copy-start.7
  46.4 2.9 copy-start.2
  49.3 31.1 %copy-start.8 = (bf16[256,2,128]{2,1,0:T(2,128)(2,1)S(1)}, bf16[256,2,128]{2,1,0:T(2,128)(2,1)}, u32[]{:S(2)}) copy-start(bf16[256,2,128]{2,1,0:T(2,128)(2,1)} %param.20) | copy-start | bytes 393220
  81.0 1.0 copy-start.6
  83.8 1.0 copy-start.6
  87.2 2.6 copy-start.11
  87.2 2.6 copy-start.13
  87.2 2.6 copy-start.14
  87.2 2.8 copy-start.15
  89.9 1.2 copy-start.5
  91.2 1.5 copy-start.12
  91.2 26.5 %copy-start.3 = (bf16[64,2048]{1,0:T(8,128)(2,1)S(1)}, bf16[64,2048]{1,0:T(8,128)(2,1)}, u32[]{:S(2)}) copy-start(bf16[64,2048]{1,0:T(8,128)(2,1)} %param.19) | copy-start | bytes 786436
  92.6 44.8 %all-gather.4.cloned.1.call-start = ((), (), s32[]{:S(2)}) async-start(), calls=%async_computation.3 | async-start | bytes 1310720 | tf_op jit(solution)/shard_map/all_gather | solution.py:145
  120.6 168.1 %all-gather.6.cloned.1.call-start = ((), (), s32[]{:S(2)}) async-start(), calls=%async_computation.4 | async-start | bytes 10485760 | tf_op jit(solution)/shard_map/all_gather | solution.py:146
  121.3 316.6 %all-gather.8.cloned.1.call-start = ((), (), s32[]{:S(2)}) async-start(), calls=%async_computation.5 | async-start | bytes 10485760 | tf_op jit(solution)/shard_map/all_gather | solution.py:151
  121.9 350.7 %copy-start.4 = (bf16[64,2048]{1,0:T(8,128)(2,1)S(1)}, bf16[64,2048]{1,0:T(8,128)(2,1)}, u32[]{:S(2)}) copy-start(bf16[64,2048]{1,0:T(8,128)(2,1)} %reduce-scatter.3.cloned.1.call-done) | copy-start | bytes 786436
  121.9 350.7 %reduce-scatter.5.cloned.1.call-start = ((), (), s32[]{:S(2)}) async-start(), calls=%async_computation.6 | async-start | bytes 1310720 | tf_op jit(solution)/shard_map/reduce_scatter | solution.py:154
Sparse Core Ops, SparseCore 0:
  92.7 24.8 reduce-scatter.2
  120.7 16.6 all-gather.3
  139.0 149.6 all-gather.5
  290.1 147.7 all-gather.7
  449.6 22.9 reduce-scatter.4
where the time goes:
time: 481 us
  waiting for transfers between devices  365 us (76%)
  blocking collectives  62.9 us (13%)
  matrix products  22.6 us (5%)
  between operations  13.4 us (3%)
  local copies, waits for them, and re-layouts  9.51 us (2%)
  other arithmetic  6.74 us (1%)
    all_gather x1, waiting for transfers between devices, shards(): up_collected = lax.all_gather(up_weight, 'sp', axis=0, tiled=True)  151 us
    all_gather x1, waiting for transfers between devices, shards(): lax.all_gather(down_weight, 'sp', axis=1, tiled=True)  149 us
    reduce_scatter x1, waiting for transfers between devices, shards(): lax.psum_scatter((jnp.dot(att_narrow, out_narrow, preferred_element_type=...  25 us
    reduce_scatter x1, waiting for transfers between devices, shards(): lax.psum_scatter(partials.astype(jnp.bfloat16), 'tp', scatter_dimension=0...  23.1 us
    all_gather x1, blocking collectives, attend(): wide_keys = lax.all_gather(key_wide, 'sp', axis=0, tiled=True)  17.7 us
    all_gather x1, blocking collectives, attend(): narrow_values = lax.all_gather(value_narrow, 'sp', axis=0, tiled=True)  15.6 us
    all_gather x1, waiting for transfers between devices, shards(): whole_rows = lax.all_gather(normed, 'tp', axis=0, tiled=True)  15.5 us
    all_gather x1, blocking collectives, attend(): wide_values = lax.all_gather(value_wide, 'sp', axis=0, tiled=True)  15.3 us
  transfers between devices with their start and end apart: 5, of which 5 were waited for; matrix products, arithmetic and copies ran while one was open for 0% of the time, Pallas kernels for 0%

commit v1 on v0

--- a/solution.py
+++ b/solution.py
@@ -3,6 +3,8 @@
 import jax
 import jax.numpy as jnp
 from jax import lax
+from jax.experimental import pallas as pl
+from jax.experimental.pallas import tpu as pltpu
 from jax.sharding import PartitionSpec as P
 
 NORM_EPS = 1e-06
@@ -157,6 +159,325 @@
     return (middle_f32 + mixer_out).astype(jnp.bfloat16)
 
 
+LOG2E = math.log2(math.e)
+VMEM_BYTES = 60 * 2**20
+
+
+def dot32(a, b):
+    return jnp.dot(a, b, preferred_element_type=jnp.float32)
+
+
+def layer_kernel(plan, resid, q, kv, lam_n, lam_w, head_gain, out_n, out_w, norm_gain, up, down,
+                 out, kv_full, att, proj_send, proj_recv, middle, act, up_full, down_full,
+                 part, core_recv, x_send, x_recv, z_send, z_recv, total,
+                 kv_ss, kv_rs, wz_ss, wz_rs, wy_ss, wy_rs, wl_sem, p_ss, p_rs,
+                 az_ss, az_rs, ax_ss, ax_rs, ac_ss, ac_rs,
+                 rc_ss, rc_rs, rx_ss, rx_rs, rz_ss, rz_rs):
+    grp_n, sp_n, tp_n, maps = plan
+    g, s, t = lax.axis_index("grp"), lax.axis_index("sp"), lax.axis_index("tp")
+    rows = kv.shape[0]
+    mine = resid.shape[0]
+    width = resid.shape[1]
+    deep = up.shape[0]
+    hid = up_full.shape[1]
+    f32, bf16 = jnp.float32, jnp.bfloat16
+
+    def ahead(d):
+        return lax.rem(s + d, sp_n)
+
+    def behind(d):
+        return lax.rem(s + sp_n - d, sp_n)
+
+    x_peer = lax.rem(t + 2, tp_n)
+    c_peer = t + 1 - 2 * lax.rem(t, 2)
+    y_peer = 1 - g
+
+    def send(src, dst, ss, rs, dev):
+        copy = pltpu.make_async_remote_copy(
+            src_ref=src, dst_ref=dst, send_sem=ss, recv_sem=rs,
+            device_id=dev, device_id_type=pl.DeviceIdType.MESH)
+        return copy
+
+    barrier = pltpu.get_barrier_semaphore()
+    peers = [{"sp": ahead(d)} for d in range(1, sp_n)]
+    peers += [{"tp": lax.rem(t + d, tp_n)} for d in range(1, tp_n)]
+    peers += [{"grp": y_peer}]
+    for peer in peers:
+        pl.semaphore_signal(barrier, inc=1, device_id=peer, device_id_type=pl.DeviceIdType.MESH)
+    pl.semaphore_wait(barrier, len(peers))
+
+    kv_copy = []
+    for d in range(1, sp_n):
+        copy = send(kv, kv_full.at[pl.ds(s * rows, rows)], kv_ss.at[d], kv_rs.at[d], {"sp": ahead(d)})
+        copy.start()
+        kv_copy.append(copy)
+
+    half_d, half_h = deep // grp_n, hid // grp_n
+    wz = []
+    for d in range(1, sp_n):
+        to = ahead(d)
+        pair = (
+            send(up.at[pl.ds(g * half_d, half_d), pl.ds(pl.multiple_of(to * hid, 128), hid)],
+                 up_full.at[pl.ds(s * deep + g * half_d, half_d)],
+                 wz_ss.at[0, d], wz_rs.at[0, d], {"sp": to}),
+            send(down.at[pl.ds(to * hid + g * half_h, half_h)],
+                 down_full.at[pl.ds(g * half_h, half_h), pl.ds(pl.multiple_of(s * deep, 128), deep)],
+                 wz_ss.at[1, d], wz_rs.at[1, d], {"sp": to}),
+        )
+        for copy in pair:
+            copy.start()
+        wz.append(pair)
+    own_up = pltpu.make_async_copy(
+        up.at[:, pl.ds(pl.multiple_of(s * hid, 128), hid)], up_full.at[pl.ds(s * deep, deep)], wl_sem.at[0])
+    own_down = pltpu.make_async_copy(
+        down.at[pl.ds(s * hid, hid)], down_full.at[:, pl.ds(pl.multiple_of(s * deep, 128), deep)], wl_sem.at[1])
+    own_up.start()
+    own_down.start()
+
+    kv_full[pl.ds(s * rows, rows)] = kv[...]
+    for copy in kv_copy:
+        copy.wait_recv()
+
+    for h, (pair, lam_of, v_at, scale) in enumerate(maps):
+        lam = (lam_n if lam_of[0] == 0 else lam_w)[lam_of[1]]
+        sides = []
+        for q_at, k_at, k_width in pair:
+            scores = lax.dot_general(
+                q[:, q_at:q_at + k_width], kv_full[:, k_at:k_at + k_width],
+                (((1,), (1,)), ((), ())), preferred_element_type=f32)
+            top = jnp.max(scores, axis=-1, keepdims=True)
+            powers = jnp.exp2((scores - top) * (scale * LOG2E))
+            row_total = jnp.sum(powers, axis=-1, keepdims=True)
+            vals = kv_full[:, v_at:v_at + head_gain.shape[1]]
+            sides.append(dot32(powers.astype(bf16), vals) / row_total)
+        mixed = sides[0] - lam * sides[1]
+        v_width = mixed.shape[1]
+        normed = (mixed * lax.rsqrt(jnp.mean(mixed * mixed, axis=-1, keepdims=True) + NORM_EPS)
+                  * head_gain[...] * OUT_SCALE)
+        att[:, h * v_width:(h + 1) * v_width] = normed.astype(bf16)
+
+    cut = out_n.shape[0]
+    chunk = math.gcd(width, 512)
+
+    @pl.loop(0, width // chunk)
+    def _(j):
+        cols = pl.ds(pl.multiple_of(j * chunk, chunk), chunk)
+        proj_send[:, cols] = (dot32(att[:, :cut], out_n[:, cols]) + dot32(att[:, cut:], out_w[:, cols])).astype(bf16)
+
+    p_copy = []
+    for d in (2, 3, 1):
+        to = lax.rem(t + d, tp_n)
+        copy = send(proj_send.at[pl.ds(to * mine, mine)], proj_recv.at[d], p_ss.at[d], p_rs.at[d], {"tp": to})
+        copy.start()
+        p_copy.append(copy)
+
+    wy = []
+
+    def forward_weights(d):
+        for copy in wz[d - 1]:
+            copy.wait_recv()
+        at = behind(d)
+        a = up_full.at[pl.ds(at * deep + g * half_d, half_d)]
+        b = down_full.at[pl.ds(g * half_h, half_h), pl.ds(pl.multiple_of(at * deep, 128), deep)]
+        for kind, ref in enumerate((a, b)):
+            copy = send(ref, ref, wy_ss.at[kind, d], wy_rs.at[kind, d], {"grp": y_peer})
+            copy.start()
+            wy.append(copy)
+
+    forward_weights(1)
+    for copy in p_copy:
+        copy.wait_recv()
+    projected = proj_send[pl.ds(t * mine, mine)].astype(f32)
+    for d in range(1, tp_n):
+        projected = projected + proj_recv[d].astype(f32)
+    mid = (resid[...].astype(f32) + projected).astype(bf16)
+    middle[...] = mid
+    mid32 = mid.astype(f32)
+    normed = mid32 * lax.rsqrt(jnp.mean(mid32 * mid32, axis=-1, keepdims=True) + NORM_EPS)
+
+    def block(z, who):
+        return act.at[pl.ds(z * rows + who * mine, mine)]
+
+    act[pl.ds(s * rows + t * mine, mine)] = (normed * norm_gain[...].astype(f32)).astype(bf16)
+
+    az, ax, ac = [], [], []
+    for d in range(1, sp_n):
+        copy = send(block(s, t), block(s, t), az_ss.at[d], az_rs.at[d], {"sp": ahead(d)})
+        copy.start()
+        az.append(copy)
+
+    def spread(d):
+        if d:
+            az[d - 1].wait_recv()
+        ref = block(behind(d), t)
+        a = send(ref, ref, ax_ss.at[d], ax_rs.at[d], {"tp": x_peer})
+        a.start()
+        ax.append(a)
+        c = send(ref, ref, ac_ss.at[0, d], ac_rs.at[0, d], {"tp": c_peer})
+        c.start()
+        ac.append([c])
+
+    spread(0)
+    for d in range(2, sp_n):
+        forward_weights(d)
+    own_up.wait()
+    own_down.wait()
+    for copy in wy:
+        copy.wait_recv()
+
+    rc, rx, rz = [], [], []
+
+    def compute(d):
+        ax[d].wait_recv()
+        ref = block(behind(d), x_peer)
+        c = send(ref, ref, ac_ss.at[1, d], ac_rs.at[1, d], {"tp": c_peer})
+        c.start()
+        ac[d].append(c)
+        if d + 1 < sp_n:
+            spread(d + 1)
+        for copy in ac[d]:
+            copy.wait_recv()
+        lifted = dot32(act[pl.ds(behind(d) * rows, rows)], up_full[...])
+        hidden = jnp.square(jnp.maximum(lifted, 0.0)).astype(bf16)
+
+        @pl.loop(0, width // chunk)
+        def _(j):
+            cols = pl.ds(pl.multiple_of(j * chunk, chunk), chunk)
+            part[d, :, cols] = dot32(hidden, down_full[:, cols]).astype(bf16)
+
+        pair = []
+        for i, who in enumerate((c_peer, lax.rem(c_peer + 2, tp_n))):
+            copy = send(part.at[d, pl.ds(who * mine, mine)], core_recv.at[d, i], rc_ss.at[d, i], rc_rs.at[d, i],
+                        {"tp": c_peer})
+            copy.start()
+            pair.append(copy)
+        rc.append(pair)
+
+    def across(d):
+        for copy in rc[d]:
+            copy.wait_recv()
+        x_send[d] = (part[d, pl.ds(x_peer * mine, mine)].astype(f32) + core_recv[d, 1].astype(f32)).astype(bf16)
+        copy = send(x_send.at[d], x_recv.at[d], rx_ss.at[d], rx_rs.at[d], {"tp": x_peer})
+        copy.start()
+        rx.append(copy)
+
+    def home(d):
+        rx[d].wait_recv()
+        term = (part[d, pl.ds(t * mine, mine)].astype(f32) + core_recv[d, 0].astype(f32)
+                + x_recv[d].astype(f32))
+        if d == 0:
+            total[...] = term
+            return
+        z_send[d] = term.astype(bf16)
+        copy = send(z_send.at[d], z_recv.at[d], rz_ss.at[d], rz_rs.at[d], {"sp": behind(d)})
+        copy.start()
+        rz.append(copy)
+
+    for step in range(sp_n + 2):
+        if step < sp_n:
+            compute(step)
+        if 0 <= step - 1 < sp_n:
+            across(step - 1)
+        if 0 <= step - 2 < sp_n:
+            home(step - 2)
+    mixer = total[...]
+    for copy in rz:
+        copy.wait_recv()
+    for d in range(1, sp_n):
+        mixer = mixer + z_recv[d].astype(f32)
+    out[...] = (middle[...].astype(f32) + mixer).astype(bf16)
+    sent = kv_copy + [c for pair in wz for c in pair] + p_copy + wy + az + ax
+    sent += [c for pair in ac for c in pair] + [c for pair in rc for c in pair] + rx + rz
+    for copy in sent:
+        copy.wait_send()
+
+
+def split_maps(query, masked):
+    row_count, heads, both = query.shape
+    half = both // 2
+    if not masked:
+        return query.reshape(row_count, heads * both)
+    zero = jnp.zeros_like(query[:, :, :half])
+    first = jnp.concatenate([query[:, :, :half], zero], axis=-1)
+    second = jnp.concatenate([zero, query[:, :, half:]], axis=-1)
+    return jnp.stack([first, second], axis=2).reshape(row_count, heads * 2 * both)
+
+
+def fused(sizes, resid_in, query_narrow, key_narrow, value_narrow, query_wide, key_wide, value_wide,
+          lambda_narrow, lambda_wide, head_gain, out_narrow, out_wide, norm_gain, up_weight, down_weight):
+    grp_n, sp_n, tp_n = sizes
+    bf16, f32 = jnp.bfloat16, jnp.float32
+    q_parts, kv_parts, maps = [], [], []
+    q_at = kv_at = 0
+    for kind, (query, key, value) in enumerate(
+            ((query_narrow, key_narrow, value_narrow), (query_wide, key_wide, value_wide))):
+        rows, heads, both = query.shape
+        kheads, v_width = key.shape[1], value.shape[2]
+        half = both // 2
+        masked = half % 128 != 0
+        q_parts.append(split_maps(query, masked))
+        kv_parts += [key.reshape(rows, kheads * both), value.reshape(rows, kheads * v_width)]
+        for h in range(heads):
+            kh = h // (heads // kheads)
+            k0 = kv_at + kh * both
+            v0 = kv_at + kheads * both + kh * v_width
+            if masked:
+                pair = tuple((q_at + (2 * h + c) * both, k0, both) for c in range(2))
+            else:
+                pair = tuple((q_at + h * both + c * half, k0 + c * half, half) for c in range(2))
+            maps.append((pair, (kind, h), v0, half ** -0.5))
+        q_at += q_parts[-1].shape[1]
+        kv_at += kheads * (both + v_width)
+    q = jnp.concatenate(q_parts, axis=1)
+    kv = jnp.concatenate(kv_parts, axis=1)
+    mine, width = resid_in.shape
+    deep, hid = up_weight.shape[0], up_weight.shape[1] // sp_n
+    vm, sm, anyw = (pl.BlockSpec(memory_space=m) for m in (pltpu.VMEM, pltpu.SMEM, pl.ANY))
+    dma = pltpu.SemaphoreType.DMA
+    n = sp_n
+    scratch = [
+        pltpu.VMEM((n * rows, kv.shape[1]), bf16),
+        pltpu.VMEM((rows, len(maps) * v_width), bf16),
+        pltpu.VMEM((rows, width), bf16),
+        pltpu.VMEM((tp_n, mine, width), bf16),
+        pltpu.VMEM((mine, width), bf16),
+        pltpu.VMEM((n * rows, width), bf16),
+        pltpu.VMEM((width, hid), bf16),
+        pltpu.VMEM((hid, width), bf16),
+        pltpu.VMEM((n, rows, width), bf16),
+        pltpu.VMEM((n, 2, mine, width), bf16),
+        pltpu.VMEM((n, mine, width), bf16),
+        pltpu.VMEM((n, mine, width), bf16),
+        pltpu.VMEM((n, mine, width), bf16),
+        pltpu.VMEM((n, mine, width), bf16),
+        pltpu.VMEM((mine, width), f32),
+        dma((n,)), dma((n,)),
+        dma((2, n)), dma((2, n)), dma((2, n)), dma((2, n)), dma((2,)),
+        dma((tp_n,)), dma((tp_n,)),
+        dma((n,)), dma((n,)), dma((n,)), dma((n,)), dma((2, n)), dma((2, n)),
+        dma((n, 2)), dma((n, 2)), dma((n,)), dma((n,)), dma((n,)), dma((n,)),
+    ]
+    return pl.pallas_call(
+        lambda *refs: layer_kernel((grp_n, sp_n, tp_n, tuple(maps)), *refs),
+        out_shape=jax.ShapeDtypeStruct(resid_in.shape, bf16),
+        in_specs=[vm, vm, vm, sm, sm, vm, vm, vm, vm, anyw, anyw],
+        out_specs=vm,
+        scratch_shapes=scratch,
+        compiler_params=pltpu.CompilerParams(
+            collective_id=0, has_side_effects=True, vmem_limit_bytes=VMEM_BYTES),
+        name="layer",
+    )(resid_in, q, kv, lambda_narrow, lambda_wide, head_gain[None], out_narrow, out_wide,
+      norm_gain[None], up_weight, down_weight)
+
+
+def fits(sizes, resid_in, query_narrow, up_weight):
+    grp_n, sp_n, tp_n = sizes
+    rows, width = query_narrow.shape[0], resid_in.shape[1]
+    held = 2 * width * (3 * sp_n * rows + 2 * rows + 2 * up_weight.shape[1] // sp_n)
+    return (grp_n == 2 and tp_n == 4 and up_weight.shape[1] % (sp_n * 256) == 0
+            and up_weight.shape[0] % 256 == 0 and held < VMEM_BYTES // 2)
+
+
 def solution(mesh):
     placed = (
         P(("grp", "sp", "tp"), None),
@@ -175,6 +496,13 @@
         P("sp", "tp"),
         P("tp", "sp"),
     )
+    sizes = tuple(mesh.shape[axis] for axis in ("grp", "sp", "tp"))
+
+    def layer(*blocks):
+        if fits(sizes, blocks[0], blocks[1], blocks[13]):
+            return fused(sizes, *blocks)
+        return shards(*blocks)
+
     return jax.shard_map(
-        shards, mesh=mesh, in_specs=placed, out_specs=P(("grp", "sp", "tp"), None), check_vma=False
-    )
+        layer, mesh=mesh, in_specs=placed, out_specs=P(("grp", "sp", "tp"), None), check_vma=False
+    )

time: 481 us -> 174 us (0.36)
  waiting for transfers between devices: 365 us -> 0 us
  Pallas kernels: 0 us -> 166 us
  blocking collectives: 62.9 us -> 0 us
  matrix products: 22.6 us -> 0 us
  between operations: 13.4 us -> 0.06 us
    all_gather x3 -> x0, waiting for transfers between devices: 316 us -> none  [the longest x1 151 us: shards(): up_collected = lax.all_gather(up_weight, 'sp', axis=0, tiled=True)]
    pallas_call x0 -> x1, Pallas kernels: none -> 166 us  [fused(): pl.pallas_call(lambda *refs: layer_kernel((grp_n, sp_n, tp_n, tuple(maps)...]
    all_gather x4 -> x0, blocking collectives: 62.9 us -> none  [the longest x1 17.7 us: attend(): wide_keys = lax.all_gather(key_wide, 'sp', axis=0, tiled=True)]
    reduce_scatter x2 -> x0, waiting for transfers between devices: 48.1 us -> none  [the longest x1 25 us: shards(): lax.psum_scatter((jnp.dot(att_narrow, out_narrow, preferred_element_type=...]
    dot_general x11 -> x0, matrix products: 22.6 us -> none  [the longest x1 11.5 us: shards(): jnp.dot(activated, lax.all_gather(down_weight, 'sp', axis=1, tiled=True),...]
    while x22 -> x0, local copies, waits for them, and re-layouts: 5.75 us -> none
  transfers between devices with their start and end apart: 5 -> 0, of which waited for: 5 -> 0; matrix products, arithmetic and copies ran while one was open for 0% -> 0% of each run, Pallas kernels for 0% -> 0%
where the time goes in v1:
time: 174 us
  Pallas kernels  166 us (95%)
  local copies, waits for them, and re-layouts  4.7 us (3%)
  other arithmetic  3.22 us (2%)
    pallas_call x1, Pallas kernels, fused(): pl.pallas_call(lambda *refs: layer_kernel((grp_n, sp_n, tp_n, tuple(maps)...  166 us

profile of v1, /device:TPU:0, one launch (start us, length us, event | category | flops | bytes accessed | tf_op | source)
XLA Modules:
  0.0 174.2 jit_solution(16184281348972579312)
XLA Ops:
  0.0 0.0 copy-start.2
  0.0 0.0 copy-start.1
  0.0 0.0 copy-start
  0.0 0.0 copy-start.3
  0.0 0.0 copy-start.4
  0.0 1.4 broadcast_in_dim.8.refs_8_
  1.4 1.1 slice.5
  2.5 1.2 fusion
  3.7 0.4 pad_maximum_fusion.2
  4.1 0.4 copy.16
  4.5 0.1 reshape.18
  4.6 0.0 copy-done
  4.7 0.9 pad_maximum_fusion.refs_1_
  5.5 0.0 copy-done.2
  5.5 0.0 copy-done.1
  5.5 0.0 copy-done.3
  5.5 0.0 copy-done.4
  5.5 0.8 pad_maximum_fusion.1.refs_2_
  6.3 166.2 %layer.1 = bf16[64,2048]{1,0:T(8,128)(2,1)} custom-call(bf16[64,2048]{1,0:T(8,128)(2,1)} %refs_0_.1, bf16[256,1024]{1,0:T(8,128)(2,1)} %pad_maximum_fusion.refs_1_, bf16[256,640]{1,0:T(8,128)(2,1)} %pad_maximum_fusion.1.refs_2_, f32[2]{0:T(128)} %refs_3_.1, f32[2]{0:T(128)} %refs_4_.1, f32[1,128]{1,0:T(1,128)} %bitcast.17, bf16[256,2048]{1,0:T(8,128)(2,1)} %refs_6_.1, ...), custom_call_target="tpu_custom_call" | custom-call | tf_op jit(solution)/shard_map/layer/pallas_call | solution.py:460
  172.5 1.7 copy.19
  (1 shorter events, 0.0 us)
Async XLA Ops:
  0.0 5.5 %copy-start.2 = (bf16[256,1,128]{2,0,1:T(8,128)(2,1)S(1)}, bf16[256,1,128]{2,0,1:T(8,128)(2,1)}, u32[]{:S(2)}) copy-start(bf16[256,1,128]{2,0,1:T(8,128)(2,1)} %param.21) | copy-start | bytes 196612
  0.0 5.5 %copy-start.1 = (bf16[256,1,256]{2,0,1:T(8,128)(2,1)S(1)}, bf16[256,1,256]{2,0,1:T(8,128)(2,1)}, u32[]{:S(2)}) copy-start(bf16[256,1,256]{2,0,1:T(8,128)(2,1)} %param.20) | copy-start | bytes 393220
  0.0 4.6 %copy-start = (bf16[256,2,256]{2,1,0:T(2,128)(2,1)S(1)}, bf16[256,2,256]{2,1,0:T(2,128)(2,1)}, u32[]{:S(2)}) copy-start(bf16[256,2,256]{2,1,0:T(2,128)(2,1)} %param.19) | copy-start | bytes 786436
  0.0 5.5 %copy-start.3 = (bf16[256,1,128]{2,0,1:T(8,128)(2,1)S(1)}, bf16[256,1,128]{2,0,1:T(8,128)(2,1)}, u32[]{:S(2)}) copy-start(bf16[256,1,128]{2,0,1:T(8,128)(2,1)} %param.18) | copy-start | bytes 196612
  0.0 5.5 %copy-start.4 = (bf16[256,1,128]{2,0,1:T(8,128)(2,1)S(1)}, bf16[256,1,128]{2,0,1:T(8,128)(2,1)}, u32[]{:S(2)}) copy-start(bf16[256,1,128]{2,0,1:T(8,128)(2,1)} %param.17) | copy-start | bytes 196612

commit v2 on v1

--- a/solution.py
+++ b/solution.py
@@ -206,12 +206,6 @@
         pl.semaphore_signal(barrier, inc=1, device_id=peer, device_id_type=pl.DeviceIdType.MESH)
     pl.semaphore_wait(barrier, len(peers))
 
-    kv_copy = []
-    for d in range(1, sp_n):
-        copy = send(kv, kv_full.at[pl.ds(s * rows, rows)], kv_ss.at[d], kv_rs.at[d], {"sp": ahead(d)})
-        copy.start()
-        kv_copy.append(copy)
-
     half_d, half_h = deep // grp_n, hid // grp_n
     wz = []
     for d in range(1, sp_n):
@@ -224,8 +218,6 @@
                  down_full.at[pl.ds(g * half_h, half_h), pl.ds(pl.multiple_of(s * deep, 128), deep)],
                  wz_ss.at[1, d], wz_rs.at[1, d], {"sp": to}),
         )
-        for copy in pair:
-            copy.start()
         wz.append(pair)
     own_up = pltpu.make_async_copy(
         up.at[:, pl.ds(pl.multiple_of(s * hid, 128), hid)], up_full.at[pl.ds(s * deep, deep)], wl_sem.at[0])
@@ -234,9 +226,45 @@
     own_up.start()
     own_down.start()
 
-    kv_full[pl.ds(s * rows, rows)] = kv[...]
-    for copy in kv_copy:
-        copy.wait_recv()
+    def passing(k, way):
+        at = pl.ds((s - way * k) * rows, rows)
+        lane = (1 - way) // 2
+        return send(kv if k == 0 else kv_full.at[at], kv_full.at[at], kv_ss.at[lane, k], kv_rs.at[lane, k],
+                    {"sp": s + way})
+
+    def arriving(k, way):
+        at = pl.ds((s - way * k) * rows, rows)
+        lane = (1 - way) // 2
+        return send(kv, kv_full.at[at], kv_ss.at[lane, k - 1], kv_rs.at[lane, k - 1], {"sp": s})
+
+    def passes(k, way):
+        return (s >= k) & (s < sp_n - 1) if way == 1 else (s <= sp_n - 1 - k) & (s > 0)
+
+    for k in range(sp_n):
+        for way in (1, -1):
+            @pl.when((s >= k) if way == 1 else (s <= sp_n - 1 - k))
+            def _():
+                if k:
+                    arriving(k, way).wait_recv()
+
+            @pl.when(passes(k, way))
+            def _():
+                passing(k, way).start()
+
+        @pl.when(s == k)
+        def _():
+            for d in range(1, sp_n - k):
+                for copy in wz[d - 1]:
+                    copy.start()
+
+        @pl.when(s == sp_n - 1 - k)
+        def _():
+            for d in range(k + 1, sp_n):
+                for copy in wz[d - 1]:
+                    copy.start()
+
+        if k == 0:
+            kv_full[pl.ds(s * rows, rows)] = kv[...]
 
     for h, (pair, lam_of, v_at, scale) in enumerate(maps):
         lam = (lam_n if lam_of[0] == 0 else lam_w)[lam_of[1]]
@@ -284,7 +312,8 @@
             copy.start()
             wy.append(copy)
 
-    forward_weights(1)
+    for d in range(1, sp_n - 1):
+        forward_weights(d)
     for copy in p_copy:
         copy.wait_recv()
     projected = proj_send[pl.ds(t * mine, mine)].astype(f32)
@@ -295,99 +324,124 @@
     mid32 = mid.astype(f32)
     normed = mid32 * lax.rsqrt(jnp.mean(mid32 * mid32, axis=-1, keepdims=True) + NORM_EPS)
 
-    def block(z, who):
-        return act.at[pl.ds(z * rows + who * mine, mine)]
-
-    act[pl.ds(s * rows + t * mine, mine)] = (normed * norm_gain[...].astype(f32)).astype(bf16)
-
-    az, ax, ac = [], [], []
-    for d in range(1, sp_n):
-        copy = send(block(s, t), block(s, t), az_ss.at[d], az_rs.at[d], {"sp": ahead(d)})
+    half_rows, half_mine = rows // 2, mine // 2
+    parts = 2 * sp_n
+
+    def group(z, half):
+        return (2 * z + half) * half_rows
+
+    def block(z, half, who):
+        return act.at[pl.ds(group(z, half) + who * half_mine, half_mine)]
+
+    sealed = (normed * norm_gain[...].astype(f32)).astype(bf16)
+    for half in range(2):
+        act[pl.ds(group(s, half) + t * half_mine, half_mine)] = sealed[half * half_mine:(half + 1) * half_mine]
+
+    az, ax, ac = {}, {}, {}
+    for b in range(2, parts):
+        ref = block(s, b % 2, t)
+        az[b] = send(ref, ref, az_ss.at[b], az_rs.at[b], {"sp": ahead(b // 2)})
+        az[b].start()
+
+    def spread(b):
+        if b >= parts:
+            return
+        if b >= 2:
+            az[b].wait_recv()
+        ref = block(behind(b // 2), b % 2, t)
+        ax[b] = send(ref, ref, ax_ss.at[b], ax_rs.at[b], {"tp": x_peer})
+        ax[b].start()
+        ac[b] = [send(ref, ref, ac_ss.at[0, b], ac_rs.at[0, b], {"tp": c_peer})]
+        ac[b][0].start()
+
+    def cross(b):
+        if b >= parts:
+            return
+        ax[b].wait_recv()
+        ref = block(behind(b // 2), b % 2, x_peer)
+        copy = send(ref, ref, ac_ss.at[1, b], ac_rs.at[1, b], {"tp": c_peer})
         copy.start()
-        az.append(copy)
-
-    def spread(d):
-        if d:
-            az[d - 1].wait_recv()
-        ref = block(behind(d), t)
-        a = send(ref, ref, ax_ss.at[d], ax_rs.at[d], {"tp": x_peer})
-        a.start()
-        ax.append(a)
-        c = send(ref, ref, ac_ss.at[0, d], ac_rs.at[0, d], {"tp": c_peer})
-        c.start()
-        ac.append([c])
-
-    spread(0)
-    for d in range(2, sp_n):
-        forward_weights(d)
-    own_up.wait()
-    own_down.wait()
-    for copy in wy:
-        copy.wait_recv()
-
-    rc, rx, rz = [], [], []
-
-    def compute(d):
-        ax[d].wait_recv()
-        ref = block(behind(d), x_peer)
-        c = send(ref, ref, ac_ss.at[1, d], ac_rs.at[1, d], {"tp": c_peer})
-        c.start()
-        ac[d].append(c)
-        if d + 1 < sp_n:
-            spread(d + 1)
-        for copy in ac[d]:
+        ac[b].append(copy)
+
+    rc, rx, rz = {}, {}, []
+
+    def compute(b):
+        for copy in ac[b]:
             copy.wait_recv()
-        lifted = dot32(act[pl.ds(behind(d) * rows, rows)], up_full[...])
+        lifted = dot32(act[pl.ds(group(behind(b // 2), b % 2), half_rows)], up_full[...])
         hidden = jnp.square(jnp.maximum(lifted, 0.0)).astype(bf16)
 
         @pl.loop(0, width // chunk)
         def _(j):
             cols = pl.ds(pl.multiple_of(j * chunk, chunk), chunk)
-            part[d, :, cols] = dot32(hidden, down_full[:, cols]).astype(bf16)
-
-        pair = []
-        for i, who in enumerate((c_peer, lax.rem(c_peer + 2, tp_n))):
-            copy = send(part.at[d, pl.ds(who * mine, mine)], core_recv.at[d, i], rc_ss.at[d, i], rc_rs.at[d, i],
-                        {"tp": c_peer})
+            part[b, :, cols] = dot32(hidden, down_full[:, cols]).astype(bf16)
+
+        rc[b] = []
+        for i, who in enumerate((lax.rem(c_peer + 2, tp_n), c_peer)):
+            copy = send(part.at[b, pl.ds(who * half_mine, half_mine)], core_recv.at[b, i],
+                        rc_ss.at[b, i], rc_rs.at[b, i], {"tp": c_peer})
             copy.start()
-            pair.append(copy)
-        rc.append(pair)
-
-    def across(d):
-        for copy in rc[d]:
+            rc[b].append(copy)
+
+    def across(b):
+        if b < 0:
+            return
+        for copy in rc[b]:
             copy.wait_recv()
-        x_send[d] = (part[d, pl.ds(x_peer * mine, mine)].astype(f32) + core_recv[d, 1].astype(f32)).astype(bf16)
-        copy = send(x_send.at[d], x_recv.at[d], rx_ss.at[d], rx_rs.at[d], {"tp": x_peer})
-        copy.start()
-        rx.append(copy)
-
-    def home(d):
-        rx[d].wait_recv()
-        term = (part[d, pl.ds(t * mine, mine)].astype(f32) + core_recv[d, 0].astype(f32)
-                + x_recv[d].astype(f32))
-        if d == 0:
-            total[...] = term
+        x_send[b] = (part[b, pl.ds(x_peer * half_mine, half_mine)].astype(f32)
+                     + core_recv[b, 0].astype(f32)).astype(bf16)
+        rx[b] = send(x_send.at[b], x_recv.at[b], rx_ss.at[b], rx_rs.at[b], {"tp": x_peer})
+        rx[b].start()
+
+    def home(b):
+        if b < 0:
             return
-        z_send[d] = term.astype(bf16)
-        copy = send(z_send.at[d], z_recv.at[d], rz_ss.at[d], rz_rs.at[d], {"sp": behind(d)})
+        rx[b].wait_recv()
+        term = (part[b, pl.ds(t * half_mine, half_mine)].astype(f32) + core_recv[b, 1].astype(f32)
+                + x_recv[b].astype(f32))
+        if b < 2:
+            total[b * half_mine:(b + 1) * half_mine] = term
+            return
+        z_send[b] = term.astype(bf16)
+        copy = send(z_send.at[b], z_recv.at[b], rz_ss.at[b], rz_rs.at[b], {"sp": behind(b // 2)})
         copy.start()
         rz.append(copy)
 
-    for step in range(sp_n + 2):
-        if step < sp_n:
+    spread(0)
+    spread(1)
+    forward_weights(sp_n - 1)
+    cross(0)
+    spread(2)
+    own_up.wait()
+    own_down.wait()
+    for step in range(parts + 3):
+        spread(step + 3)
+        cross(step + 1)
+        if step == 0:
+            for copy in wy:
+                copy.wait_recv()
+        if step < parts:
             compute(step)
-        if 0 <= step - 1 < sp_n:
+        if step - 1 < parts:
             across(step - 1)
-        if 0 <= step - 2 < sp_n:
-            home(step - 2)
-    mixer = total[...]
+        if step - 3 < parts:
+            home(step - 3)
     for copy in rz:
         copy.wait_recv()
-    for d in range(1, sp_n):
-        mixer = mixer + z_recv[d].astype(f32)
-    out[...] = (middle[...].astype(f32) + mixer).astype(bf16)
-    sent = kv_copy + [c for pair in wz for c in pair] + p_copy + wy + az + ax
-    sent += [c for pair in ac for c in pair] + [c for pair in rc for c in pair] + rx + rz
+    for half in range(2):
+        at = slice(half * half_mine, (half + 1) * half_mine)
+        mixer = total[at]
+        for d in range(1, sp_n):
+            mixer = mixer + z_recv[2 * d + half].astype(f32)
+        out[at] = (middle[at].astype(f32) + mixer).astype(bf16)
+    for k in range(sp_n):
+        for way in (1, -1):
+            @pl.when(passes(k, way))
+            def _():
+                passing(k, way).wait_send()
+
+    sent = [c for pair in wz for c in pair] + p_copy + wy + list(az.values()) + list(ax.values())
+    sent += [c for pair in (*ac.values(), *rc.values()) for c in pair] + list(rx.values()) + rz
     for copy in sent:
         copy.wait_send()
 
@@ -444,18 +498,18 @@
         pltpu.VMEM((n * rows, width), bf16),
         pltpu.VMEM((width, hid), bf16),
         pltpu.VMEM((hid, width), bf16),
-        pltpu.VMEM((n, rows, width), bf16),
-        pltpu.VMEM((n, 2, mine, width), bf16),
-        pltpu.VMEM((n, mine, width), bf16),
-        pltpu.VMEM((n, mine, width), bf16),
-        pltpu.VMEM((n, mine, width), bf16),
-        pltpu.VMEM((n, mine, width), bf16),
+        pltpu.VMEM((2 * n, rows // 2, width), bf16),
+        pltpu.VMEM((2 * n, 2, mine // 2, width), bf16),
+        pltpu.VMEM((2 * n, mine // 2, width), bf16),
+        pltpu.VMEM((2 * n, mine // 2, width), bf16),
+        pltpu.VMEM((2 * n, mine // 2, width), bf16),
+        pltpu.VMEM((2 * n, mine // 2, width), bf16),
         pltpu.VMEM((mine, width), f32),
-        dma((n,)), dma((n,)),
+        dma((2, n)), dma((2, n)),
         dma((2, n)), dma((2, n)), dma((2, n)), dma((2, n)), dma((2,)),
         dma((tp_n,)), dma((tp_n,)),
-        dma((n,)), dma((n,)), dma((n,)), dma((n,)), dma((2, n)), dma((2, n)),
-        dma((n, 2)), dma((n, 2)), dma((n,)), dma((n,)), dma((n,)), dma((n,)),
+        *(dma(k) for k in ((2 * n,), (2 * n,), (2, 2 * n)) for _ in range(2)),
+        *(dma(k) for k in ((2 * n, 2), (2 * n,), (2 * n,)) for _ in range(2)),
     ]
     return pl.pallas_call(
         lambda *refs: layer_kernel((grp_n, sp_n, tp_n, tuple(maps)), *refs),
@@ -475,7 +529,7 @@
     rows, width = query_narrow.shape[0], resid_in.shape[1]
     held = 2 * width * (3 * sp_n * rows + 2 * rows + 2 * up_weight.shape[1] // sp_n)
     return (grp_n == 2 and tp_n == 4 and up_weight.shape[1] % (sp_n * 256) == 0
-            and up_weight.shape[0] % 256 == 0 and held < VMEM_BYTES // 2)
+            and up_weight.shape[0] % 256 == 0 and resid_in.shape[0] % 32 == 0 and held < VMEM_BYTES // 2)
 
 
 def solution(mesh):

time: 174 us -> 155 us (0.89)
  Pallas kernels: 166 us -> 147 us
    pallas_call x1, Pallas kernels: 166 us -> 147 us  [fused(): pl.pallas_call(lambda *refs: layer_kernel((grp_n, sp_n, tp_n, tuple(maps)...]
where the time goes in v2:
time: 155 us
  Pallas kernels  147 us (95%)
  local copies, waits for them, and re-layouts  4.7 us (3%)
  other arithmetic  3.22 us (2%)
    pallas_call x1, Pallas kernels, fused(): pl.pallas_call(lambda *refs: layer_kernel((grp_n, sp_n, tp_n, tuple(maps)...  147 us

profile of v2, /device:TPU:0, one launch (start us, length us, event | category | flops | bytes accessed | tf_op | source)
XLA Modules:
  0.0 155.2 jit_solution(6670744530660606369)
XLA Ops:
  0.0 0.0 copy-start.2
  0.0 0.0 copy-start.1
  0.0 0.0 copy-start
  0.0 0.0 copy-start.3
  0.0 0.0 copy-start.4
  0.0 1.4 broadcast_in_dim.8.refs_8_
  1.4 1.1 slice.5
  2.5 1.2 fusion
  3.7 0.4 pad_maximum_fusion.2
  4.1 0.4 copy.16
  4.5 0.1 reshape.18
  4.6 0.0 copy-done
  4.7 0.9 pad_maximum_fusion.refs_1_
  5.5 0.0 copy-done.2
  5.5 0.0 copy-done.1
  5.5 0.0 copy-done.3
  5.5 0.0 copy-done.4
  5.5 0.8 pad_maximum_fusion.1.refs_2_
  6.3 147.3 %layer.1 = bf16[64,2048]{1,0:T(8,128)(2,1)} custom-call(bf16[64,2048]{1,0:T(8,128)(2,1)} %refs_0_.1, bf16[256,1024]{1,0:T(8,128)(2,1)} %pad_maximum_fusion.refs_1_, bf16[256,640]{1,0:T(8,128)(2,1)} %pad_maximum_fusion.1.refs_2_, f32[2]{0:T(128)} %refs_3_.1, f32[2]{0:T(128)} %refs_4_.1, f32[1,128]{1,0:T(1,128)} %bitcast.17, bf16[256,2048]{1,0:T(8,128)(2,1)} %refs_6_.1, ...), custom_call_target="tpu_custom_call" | custom-call | tf_op jit(solution)/shard_map/layer/pallas_call | solution.py:514
  153.6 1.7 %copy.19 = bf16[64,2048]{1,0:T(8,128)(2,1)} copy(bf16[64,2048]{1,0:T(8,128)(2,1)} %layer.1) | data formatting | bytes 524288
  (1 shorter events, 0.0 us)
Async XLA Ops:
  0.0 5.5 %copy-start.2 = (bf16[256,1,128]{2,0,1:T(8,128)(2,1)S(1)}, bf16[256,1,128]{2,0,1:T(8,128)(2,1)}, u32[]{:S(2)}) copy-start(bf16[256,1,128]{2,0,1:T(8,128)(2,1)} %param.21) | copy-start | bytes 196612
  0.0 5.5 %copy-start.1 = (bf16[256,1,256]{2,0,1:T(8,128)(2,1)S(1)}, bf16[256,1,256]{2,0,1:T(8,128)(2,1)}, u32[]{:S(2)}) copy-start(bf16[256,1,256]{2,0,1:T(8,128)(2,1)} %param.20) | copy-start | bytes 393220
  0.0 4.6 %copy-start = (bf16[256,2,256]{2,1,0:T(2,128)(2,1)S(1)}, bf16[256,2,256]{2,1,0:T(2,128)(2,1)}, u32[]{:S(2)}) copy-start(bf16[256,2,256]{2,1,0:T(2,128)(2,1)} %param.19) | copy-start | bytes 786436
  0.0 5.5 %copy-start.3 = (bf16[256,1,128]{2,0,1:T(8,128)(2,1)S(1)}, bf16[256,1,128]{2,0,1:T(8,128)(2,1)}, u32[]{:S(2)}) copy-start(bf16[256,1,128]{2,0,1:T(8,128)(2,1)} %param.18) | copy-start | bytes 196612
  0.0 5.5 %copy-start.4 = (bf16[256,1,128]{2,0,1:T(8,128)(2,1)S(1)}, bf16[256,1,128]{2,0,1:T(8,128)(2,1)}, u32[]{:S(2)}) copy-start(bf16[256,1,128]{2,0,1:T(8,128)(2,1)} %param.17) | copy-start | bytes 196612
